TPU v7x, 128 devices: a whole 4x4x4 slice. The times are simulated.
128 devices in a mesh: ep: 128 (over z, y, x, core).
Axes of the slice: x: 4, y: 4, z: 4, core: 2. Of those that a mesh axis runs over, the one named last changes fastest.
Arguments:
- tokens: bfloat16 [2048, 2048], P('ep'), may hold values from -6 to 6
- lengths: int32 [2048], P('ep'), may hold values from 1 to 1024, 1048576 in all
- cache_keys: bfloat16 [2048, 1024, 128], P('ep'), may hold values from -6 to 6
- cache_values: bfloat16 [2048, 1024, 128], P('ep'), may hold values from -6 to 6
- mix_gain: float32 [2048], replicated, may hold values from 0.1 to 1.9
- mix_out_gain: float32 [2048], replicated, may hold values from 0.1 to 1.9
- ffn_gain: float32 [2048], replicated, may hold values from 0.1 to 1.9
- ffn_out_gain: float32 [2048], replicated, may hold values from 0.1 to 1.9
- query_weight: bfloat16 [2048, 2048], P(None, 'ep'), may hold values from -0.125 to 0.125
- key_weight: bfloat16 [2048, 128], replicated, may hold values from -0.125 to 0.125
- value_weight: bfloat16 [2048, 128], replicated, may hold values from -0.125 to 0.125
- head_bias: float32 [32], replicated, may hold values from -8 to -2
- output_weight: bfloat16 [2048, 2048], P(None, 'ep'), may hold values from -0.125 to 0.125
- routes: int32 [2048, 6], P('ep'), may hold values from 0 to 127, all different within a row; in each aligned block of 16 rows (0 to 15, 16 to 31, ...) at most 2 rows name the same one
- route_weights: float32 [2048, 6], P('ep'), may hold values from 0.1 to 1
- expert_gate: bfloat16 [128, 2048, 512], P('ep'), may hold values from -0.125 to 0.125
- expert_up: bfloat16 [128, 2048, 512], P('ep'), may hold values from -0.125 to 0.125
- expert_down: bfloat16 [128, 512, 2048], P('ep'), may hold values from -0.25 to 0.25
- shared_gate: bfloat16 [2048, 512], replicated, may hold values from -0.125 to 0.125
- shared_up: bfloat16 [2048, 512], replicated, may hold values from -0.125 to 0.125
- shared_down: bfloat16 [512, 2048], replicated, may hold values from -0.25 to 0.25
Outputs:
- layer_out: bfloat16 [2048, 2048], P('ep')
- new_keys: bfloat16 [2048, 128], P('ep')
- new_values: bfloat16 [2048, 128], P('ep')
Inputs may be any that keep to these rules, and one draw needn't show every extreme that they name: `routes`: each row names 6 different experts. Among the rows of one device no expert is named more than 2 times, a bound that some block reaches in some device's rows. `lengths`: the new token stands at this position; cache entries at this position and after are unused. Some sequence has exactly 1024.
All inputs are finite; a program needn't handle non-finite values. No bound on the sum of `lengths` on one device may be relied on, other than what follows from the above.
Results may differ from a plain program's by a relative error of at most 0.013.
Values may be sent and summed in bfloat16 or wider, within the bound.
No kernel may reach another device: no remote copies, remote signals or barrier semaphores. Data moves between devices by JAX's collectives and lax.ppermute only.
A program may use at most 128 MiB of HBM per device.

v0:
```python
import math
import jax
import jax.numpy as jnp
from jax import lax
from jax.sharding import PartitionSpec as P

HD = 64


def rms_scale(rows, gain):
    return rows * lax.rsqrt(jnp.mean(rows * rows, axis=-1, keepdims=True) + 1e-06) * gain


def later_sums(values):
    seqs, kv_heads, group, span = values.shape
    width = math.gcd(span, 128)
    count = span // width
    blocked = values.reshape(seqs, kv_heads, group, count, width)
    inner_pos = jnp.arange(width)
    upper = (inner_pos[:, None] > inner_pos[None, :]).astype(jnp.float32)
    inside = jnp.einsum("skgbj,ji->skgbi", blocked, upper, precision=lax.Precision.HIGHEST)
    totals = jnp.sum(blocked, axis=4)
    block_pos = jnp.arange(count)
    beyond = (block_pos[:, None] > block_pos[None, :]).astype(jnp.float32)
    carried = jnp.einsum("skgc,cb->skgb", totals, beyond, precision=lax.Precision.HIGHEST)
    return (inside + carried[..., None]).reshape(seqs, kv_heads, group, span)


def body(
    tokens,
    lengths,
    cache_keys,
    cache_values,
    mix_gain,
    mix_out_gain,
    ffn_gain,
    ffn_out_gain,
    query_weight,
    key_weight,
    value_weight,
    head_bias,
    output_weight,
    routes,
    route_weights,
    expert_gate,
    expert_up,
    expert_down,
    shared_gate,
    shared_up,
    shared_down,
):
    resid = tokens.astype(jnp.float32)
    normed = rms_scale(resid, mix_gain).astype(jnp.bfloat16)
    new_keys = jnp.dot(normed, key_weight, preferred_element_type=jnp.float32).astype(jnp.bfloat16)
    new_values = jnp.dot(normed, value_weight, preferred_element_type=jnp.float32).astype(
        jnp.bfloat16
    )
    queries = jnp.dot(
        normed,
        lax.all_gather(query_weight, "ep", axis=1, tiled=True),
        preferred_element_type=jnp.float32,
    ).astype(jnp.bfloat16)
    seqs, span, width = cache_keys.shape
    kv_heads = width // HD
    heads = queries.shape[1] // HD
    group = heads // kv_heads
    q_heads = queries.reshape(seqs, kv_heads, group, HD)
    k_heads = cache_keys.reshape(seqs, span, kv_heads, HD)
    v_heads = cache_values.reshape(seqs, span, kv_heads, HD)
    scores = jnp.einsum(
        "skgd,slkd->skgl", q_heads, k_heads, preferred_element_type=jnp.float32
    ) * HD ** (-0.5)
    scores = scores + head_bias.reshape(kv_heads, group)[None, :, :, None]
    valid = (jnp.arange(span)[None, :] < lengths[:, None])[:, None, None, :]
    log_beta = jax.nn.log_sigmoid(scores)
    log_keep = jnp.where(valid, log_beta - scores, 0.0)
    after = later_sums(log_keep)
    stick = jnp.where(valid, jnp.exp(log_beta + after), 0.0).astype(jnp.bfloat16)
    attended = jnp.einsum("skgl,slkd->skgd", stick, v_heads, preferred_element_type=jnp.float32)
    attended = attended.astype(jnp.bfloat16).reshape(seqs, heads * HD)
    mixed = jnp.dot(
        attended,
        lax.all_gather(output_weight, "ep", axis=1, tiled=True),
        preferred_element_type=jnp.float32,
    ).astype(jnp.bfloat16)
    resid1 = resid + rms_scale(mixed.astype(jnp.float32), mix_out_gain)
    ffn_in = rms_scale(resid1, ffn_gain).astype(jnp.bfloat16)
    devices = lax.axis_size("ep")
    top = routes.shape[1]
    experts = devices * expert_gate.shape[0]
    capacity = 2 * ((seqs * top + devices - 1) // devices)
    flat = routes.reshape(-1)
    onehot = (flat[:, None] == jnp.arange(experts)[None, :]).astype(jnp.float32)
    assign_pos = jnp.arange(flat.shape[0])
    lower = (assign_pos[:, None] > assign_pos[None, :]).astype(jnp.float32)
    earlier = jnp.dot(lower, onehot, precision=lax.Precision.HIGHEST)
    rank = jnp.sum(earlier * onehot, axis=1).astype(jnp.int32)
    slot = flat * capacity + rank
    placed = slot.reshape(seqs, top)[:, :, None] == jnp.arange(experts * capacity)[None, None, :]
    dispatch = jnp.sum(placed.astype(jnp.float32), axis=1).astype(jnp.bfloat16)
    outgoing = jnp.einsum("sc,sd->cd", dispatch, ffn_in, preferred_element_type=jnp.float32)
    outgoing = outgoing.astype(jnp.bfloat16).reshape(experts, capacity, ffn_in.shape[1])
    shared_hidden = (
        jax.nn.silu(jnp.dot(ffn_in, shared_gate, preferred_element_type=jnp.float32))
        * jnp.dot(ffn_in, shared_up, preferred_element_type=jnp.float32)
    ).astype(jnp.bfloat16)
    shared_out = jnp.dot(shared_hidden, shared_down, preferred_element_type=jnp.float32)
    incoming = lax.all_to_all(outgoing, "ep", split_axis=0, concat_axis=0, tiled=True)
    sources, count, features = incoming.shape
    rows = incoming.reshape(sources * count, features)
    hidden = (
        jax.nn.silu(jnp.dot(rows, expert_gate[0], preferred_element_type=jnp.float32))
        * jnp.dot(rows, expert_up[0], preferred_element_type=jnp.float32)
    ).astype(jnp.bfloat16)
    result = jnp.dot(hidden, expert_down[0], preferred_element_type=jnp.float32).astype(
        jnp.bfloat16
    )
    returned = lax.all_to_all(
        result.reshape(sources, count, features), "ep", split_axis=0, concat_axis=0, tiled=True
    )
    picked = jnp.take(returned.reshape(experts * capacity, -1), slot, axis=0)
    routed = jnp.sum(
        picked.astype(jnp.float32).reshape(seqs, top, -1) * route_weights[:, :, None], axis=1
    )
    layer_out = (resid1 + rms_scale(routed + shared_out, ffn_out_gain)).astype(jnp.bfloat16)
    return (layer_out, new_keys, new_values)


def solution(mesh):
    in_specs = (
        P("ep", None),
        P("ep"),
        P("ep", None, None),
        P("ep", None, None),
        P(),
        P(),
        P(),
        P(),
        P(None, "ep"),
        P(),
        P(),
        P(),
        P(None, "ep"),
        P("ep", None),
        P("ep", None),
        P("ep", None, None),
        P("ep", None, None),
        P("ep", None, None),
        P(),
        P(),
        P(),
    )
    out_specs = (P("ep", None), P("ep", None), P("ep", None))
    return jax.shard_map(body, mesh=mesh, in_specs=in_specs, out_specs=out_specs, check_vma=False)
```

profile of v0, /device:TPU:1, one launch (start us, length us, event | category | flops | bytes accessed | tf_op | source)
XLA Modules:
  0.0 238.4 jit_solution(5669032476505502544)
XLA Ops:
  7.2 0.0 copy-start
  7.2 0.0 all-gather.3.cloned.1.call-start
  7.2 0.7 all-gather.3.cloned.1.call-update
  7.9 0.0 all-gather.5.cloned.1.call-start
  8.0 0.7 all-gather.5.cloned.1.call-update
  8.7 0.7 add.115
  9.4 6.4 %copy.43 = bf16[16,1024,128]{1,2,0:T(8,128)(2,1)} copy(bf16[16,1024,128]{2,1,0:T(8,128)(2,1)} %param.23) | data formatting | bytes 8388608 | tf_op args[2]
  15.8 6.5 %copy.46 = bf16[16,1024,128]{1,2,0:T(8,128)(2,1)} copy(bf16[16,1024,128]{2,1,0:T(8,128)(2,1)} %param.24) | data formatting | bytes 8388608 | tf_op args[3]
  22.3 0.0 copy-done.9
  22.3 0.1 copy.47
  22.4 0.1 reshape.156
  22.5 0.3 fusion.13
  22.8 0.1 convert_element_type.88
  22.9 0.1 copy.49
  23.0 0.1 convert_reduce_fusion
  23.1 0.0 copy-done.1
  23.1 0.1 fusion.26
  23.2 0.0 copy-done.11
  23.2 0.1 iota_compare_fusion.2
  23.3 61.0 %all-gather.3.cloned.1.call-done = bf16[2048,2048]{0,1:T(8,128)(2,1)} async-done(((bf16[2048,16]{0,1:T(8,128)(2,1)}), bf16[2048,2048]{0,1:T(8,128)(2,1)}) %all-gather.3.cloned.1.call-update) | async-done | bytes 8388624 | tf_op jit(solution)/shard_map/all_gather | solution.py:60
  84.3 0.0 copy-done.5
  84.3 5.6 %convolution_convert_fusion.3 = bf16[16,2048]{1,0:T(8,128)(2,1)S(1)} fusion(bf16[2048,2048]{0,1:T(8,128)(2,1)} %all-gather.3.cloned.1.call-done, bf16[16,2048]{1,0:T(8,128)(2,1)S(1)} %copy-done.1, f32[2048]{0:T(1024)S(1)} %copy-done.5, f32[16]{0:T(128)S(1)} %add_rsqrt_fusion.3), kind=kOutput, calls=%fused_computation.7 | convolution fusion | flops 134381568 | bytes 8527936 | tf_op jit(solution)/shard_map/dot_general | solution.py:58
  90.0 0.2 reshape.150
  90.2 5.3 %subtract_select_fusion = (f32[16,2,16,1024]{3,2,1,0:T(8,128)S(1)}, f32[16,2,16,1024]{3,2,1,0:T(8,128)}) fusion(f32[2,16]{1,0:T(2,128)S(1)} %add.115, pred[16,1024]{1,0:T(8,128)(4,1)S(1)} %iota_compare_fusion.2, bf16[16,2,16,64]{3,2,1,0:T(8,128)(2,1)S(1)} %reshape.150, bf16[16,1024,2,64]{1,3,2,0:T(8,128)(2,1)} %bitcast.64), kind=kOutput, calls=%fused_computation.15 | convolution fusion | flops 73400320 | bytes 8470656 | tf_op jit(solution)/shard_map/skgd,slkd->skgl/dot_general | solution.py:70
  95.5 1.8 copy.55
  97.2 2.2 reduce_sum.73
  99.4 0.2 fusion.40
  99.7 4.1 %convolution_add_fusion.1 = f32[16,2,16,8,128]{4,3,2,1,0:T(8,128)} fusion(f32[16,2,16,8,128]{4,3,2,1,0:T(8,128)} %bitcast.62, f32[16,2,16,8]{3,2,1,0:T(8,128)S(1)} %fusion.40), kind=kOutput, calls=%fused_computation.17 | convolution fusion | flops 805847040 | bytes 4210688 | tf_op jit(solution)/shard_map/skgbj,ji->skgbi/dot_general | solution.py:21
  103.8 2.7 %reshape.153 = f32[16,2,16,1024]{3,2,1,0:T(8,128)} reshape(f32[16,2,16,8,128]{4,3,2,1,0:T(8,128)} %convolution_add_fusion.1) | data formatting | bytes 4194304 | tf_op jit(solution)/shard_map/reshape | solution.py:26
  106.5 5.4 %convolution_convert_fusion.4 = bf16[16,2,16,64]{3,2,1,0:T(8,128)(2,1)S(1)} fusion(bf16[16,1024,2,64]{1,3,2,0:T(8,128)(2,1)} %bitcast.63, f32[16,2,16,1024]{3,2,1,0:T(8,128)} %reshape.153, f32[16,2,16,1024]{3,2,1,0:T(8,128)} %get-tuple-element.6, f32[2,16]{1,0:T(2,128)S(1)} %add.115, pred[16,1024]{1,0:T(8,128)(4,1)S(1)} %iota_compare_fusion.2), kind=kOutput, calls=%fused_computation.20 | convolution fusion | flops 73957376 | bytes 8470656 | tf_op jit(solution)/shard_map/skgl,slkd->skgd/dot_general | solution.py:79
  111.9 0.2 reshape.155
  112.1 0.0 copy-start.6
  112.1 0.0 copy-start.7
  112.1 42.4 %all-gather.5.cloned.1.call-done = bf16[2048,2048]{0,1:T(8,128)(2,1)} async-done(((bf16[2048,16]{0,1:T(8,128)(2,1)}), bf16[2048,2048]{0,1:T(8,128)(2,1)}) %all-gather.5.cloned.1.call-update) | async-done | bytes 8388624 | tf_op jit(solution)/shard_map/all_gather | solution.py:83
  154.5 5.8 %multiply_reduce_fusion.3 = (f32[16]{0:T(128)S(1)}, f32[16,2048]{1,0:T(8,128)S(1)}) fusion(bf16[16,2048]{1,0:T(8,128)(2,1)S(1)} %reshape.155, bf16[2048,2048]{0,1:T(8,128)(2,1)} %all-gather.5.cloned.1.call-done), kind=kOutput, calls=%fused_computation.47 | convolution fusion | flops 134348784 | bytes 8585280 | tf_op jit(solution)/shard_map/dot_general | solution.py:81
  160.3 0.0 copy-done.6
  160.3 0.2 multiply_reduce_fusion.2
  160.5 0.0 copy-done.7
  160.5 0.1 multiply_convert_fusion
  160.6 0.4 convolution_convert_fusion.1
  161.1 0.0 copy-start.10
  161.1 1.5 reshape.157
  162.6 5.4 %all-to-all-start = ((bf16[128,2,2048]{2,1,0:T(2,128)(2,1)}), bf16[128,2,2048]{2,1,0:T(2,128)(2,1)S(1)}, u32[]{:S(2)}, u32[]{:S(2)}) async-start(bf16[128,2,2048]{2,1,0:T(2,128)(2,1)} %reshape.157), calls=%async_computation | async-start | bytes 2097152 | tf_op jit(solution)/shard_map/all_to_all | solution.py:108
  168.0 0.1 mul.150
  168.1 0.1 copy.50
  168.2 19.0 %all-to-all-done = bf16[128,2,2048]{2,1,0:T(2,128)(2,1)S(1)} async-done(((bf16[128,2,2048]{2,1,0:T(2,128)(2,1)}), bf16[128,2,2048]{2,1,0:T(2,128)(2,1)S(1)}, u32[]{:S(2)}, u32[]{:S(2)}) %all-to-all-start) | async-done | bytes 1048608 | tf_op jit(solution)/shard_map/all_to_all | solution.py:108
  187.2 1.2 reshape.158
  188.4 3.5 %fusion.5 = f32[256,512]{1,0:T(8,128)} fusion(bf16[256,2048]{1,0:T(8,128)(2,1)} %reshape.158, bf16[1,2048,512]{2,1,0:T(8,128)(2,1)} %param.36), kind=kOutput, calls=%fused_computation.12 | convolution fusion | flops 536870912 | bytes 3670016 | tf_op jit(solution)/shard_map/dot_general | solution.py:112
  191.9 0.0 copy-done
  191.9 4.0 %convolution_convert_fusion = bf16[256,2048]{1,0:T(8,128)(2,1)} fusion(bf16[1,512,2048]{2,1,0:T(8,128)(2,1)S(1)} %copy-done, bf16[256,2048]{1,0:T(8,128)(2,1)S(1)} %copy-done.2, bf16[1,2048,512]{2,1,0:T(8,128)(2,1)} %param.37, f32[256,512]{1,0:T(8,128)} %fusion.5), kind=kOutput, calls=%fused_computation.2 | convolution fusion | flops 1075052544 | bytes 6815744 | tf_op jit(solution)/shard_map/dot_general | solution.py:115
  195.9 2.6 %reshape.159 = bf16[128,2,2048]{2,1,0:T(2,128)(2,1)} reshape(bf16[256,2048]{1,0:T(8,128)(2,1)} %convolution_convert_fusion) | data formatting | bytes 2097152 | tf_op jit(solution)/shard_map/reshape | solution.py:119
  198.5 5.4 %all-to-all-start.1 = ((bf16[128,2,2048]{2,1,0:T(2,128)(2,1)}), bf16[128,2,2048]{2,1,0:T(2,128)(2,1)}, u32[]{:S(2)}, u32[]{:S(2)}) async-start(bf16[128,2,2048]{2,1,0:T(2,128)(2,1)} %reshape.159), calls=%async_computation.1 | async-start | bytes 2097152 | tf_op jit(solution)/shard_map/all_to_all | solution.py:118
  204.0 0.8 convolution_convert_fusion.5
  204.9 0.8 convolution_convert_fusion.6
  205.7 2.0 fusion.52
  207.7 15.3 %all-to-all-done.1 = bf16[128,2,2048]{2,1,0:T(2,128)(2,1)} async-done(((bf16[128,2,2048]{2,1,0:T(2,128)(2,1)}), bf16[128,2,2048]{2,1,0:T(2,128)(2,1)}, u32[]{:S(2)}, u32[]{:S(2)}) %all-to-all-start.1) | async-done | bytes 1048608 | tf_op jit(solution)/shard_map/all_to_all | solution.py:118
  223.0 1.5 reshape.160
  224.5 1.6 gather_fusion
  226.1 1.1 gather.7
  227.2 0.6 multiply_reduce_fusion
  227.8 0.0 copy-start.8
  227.8 3.1 %multiply_reduce_fusion.1 = (f32[16]{0:T(128)S(1)}, f32[16,2048]{1,0:T(8,128)S(1)}) fusion(f32[16,2048]{1,0:T(8,128)S(1)} %multiply_reduce_fusion, bf16[512,2048]{1,0:T(8,128)(2,1)} %param.41, bf16[16,2048]{1,0:T(8,128)(2,1)S(1)} %multiply_convert_fusion, bf16[2048,512]{1,0:T(8,128)(2,1)} %param.40, f32[16,512]{1,0:T(8,128)S(1)} %fusion.52), kind=kOutput, calls=%fused_computation.44 | convolution fusion | flops 67256304 | bytes 4554816 | tf_op jit(solution)/shard_map/dot_general | solution.py:107
  230.9 0.0 copy-done.8
  230.9 0.7 add_convert_fusion
  (20 shorter events, 0.1 us)
Async XLA Ops:
  7.2 184.7 %copy-start = (bf16[1,512,2048]{2,1,0:T(8,128)(2,1)S(1)}, bf16[1,512,2048]{2,1,0:T(8,128)(2,1)}, u32[]{:S(2)}) copy-start(bf16[1,512,2048]{2,1,0:T(8,128)(2,1)} %param.38) | copy-start | bytes 6291460
  7.2 77.1 %all-gather.3.cloned.1.call-start = ((), (), s32[]{:S(2)}) async-start(), calls=%async_computation.2 | async-start | bytes 8454144 | tf_op jit(solution)/shard_map/all_gather | solution.py:60
  7.9 146.6 %all-gather.5.cloned.1.call-start = ((), (), s32[]{:S(2)}) async-start(), calls=%async_computation.3 | async-start | bytes 8454144 | tf_op jit(solution)/shard_map/all_gather | solution.py:83
  15.8 6.5 %copy-start.9 = (s32[16,6]{0,1:T(8,128)S(1)}, s32[16,6]{0,1:T(8,128)}, u32[]{:S(2)}) copy-start(s32[16,6]{0,1:T(8,128)} %param.34) | copy-start | bytes 1156
  15.8 7.3 %copy-start.1 = (bf16[16,2048]{1,0:T(8,128)(2,1)S(1)}, bf16[16,2048]{1,0:T(8,128)(2,1)}, u32[]{:S(2)}) copy-start(bf16[16,2048]{1,0:T(8,128)(2,1)} %param.21) | copy-start | bytes 196612
  15.8 7.4 %copy-start.11 = (s32[16]{0:T(128)S(1)}, s32[16]{0:T(128)}, u32[]{:S(2)}) copy-start(s32[16]{0:T(128)} %param.22) | copy-start | bytes 196
  15.8 68.5 %copy-start.5 = (f32[2048]{0:T(1024)S(1)}, f32[2048]{0:T(1024)}, u32[]{:S(2)}) copy-start(f32[2048]{0:T(1024)} %param.25) | copy-start | bytes 24580
  112.1 48.2 %copy-start.6 = (f32[2048]{0:T(1024)S(1)}, f32[2048]{0:T(1024)}, u32[]{:S(2)}) copy-start(f32[2048]{0:T(1024)} %param.26) | copy-start | bytes 24580
  112.1 48.4 %copy-start.7 = (f32[2048]{0:T(1024)S(1)}, f32[2048]{0:T(1024)}, u32[]{:S(2)}) copy-start(f32[2048]{0:T(1024)} %param.27) | copy-start | bytes 24580
  161.1 7.0 %copy-start.10 = (f32[16,6]{0,1:T(8,128)S(1)}, f32[16,6]{0,1:T(8,128)}, u32[]{:S(2)}) copy-start(f32[16,6]{0,1:T(8,128)} %param.35) | copy-start | bytes 1156
  162.6 24.6 %all-to-all-start = ((bf16[128,2,2048]{2,1,0:T(2,128)(2,1)}), bf16[128,2,2048]{2,1,0:T(2,128)(2,1)S(1)}, u32[]{:S(2)}, u32[]{:S(2)}) async-start(bf16[128,2,2048]{2,1,0:T(2,128)(2,1)} %reshape.157), calls=%async_computation | async-start | bytes 2097152 | tf_op jit(solution)/shard_map/all_to_all | solution.py:108
  188.4 3.5 %copy-start.2 = (bf16[256,2048]{1,0:T(8,128)(2,1)S(1)}, bf16[256,2048]{1,0:T(8,128)(2,1)}, u32[]{:S(2)}) copy-start(bf16[256,2048]{1,0:T(8,128)(2,1)} %reshape.158) | copy-start | bytes 3145732
  195.9 8.1 %copy-start.3 = (bf16[2048,128]{1,0:T(8,128)(2,1)S(1)}, bf16[2048,128]{1,0:T(8,128)(2,1)}, u32[]{:S(2)}) copy-start(bf16[2048,128]{1,0:T(8,128)(2,1)} %param.31) | copy-start | bytes 1572868
  195.9 9.0 %copy-start.4 = (bf16[2048,128]{1,0:T(8,128)(2,1)S(1)}, bf16[2048,128]{1,0:T(8,128)(2,1)}, u32[]{:S(2)}) copy-start(bf16[2048,128]{1,0:T(8,128)(2,1)} %param.30) | copy-start | bytes 1572868
  198.5 24.5 %all-to-all-start.1 = ((bf16[128,2,2048]{2,1,0:T(2,128)(2,1)}), bf16[128,2,2048]{2,1,0:T(2,128)(2,1)}, u32[]{:S(2)}, u32[]{:S(2)}) async-start(bf16[128,2,2048]{2,1,0:T(2,128)(2,1)} %reshape.159), calls=%async_computation.1 | async-start | bytes 2097152 | tf_op jit(solution)/shard_map/all_to_all | solution.py:118
  227.8 3.1 %copy-start.8 = (f32[2048]{0:T(1024)S(1)}, f32[2048]{0:T(1024)}, u32[]{:S(2)}) copy-start(f32[2048]{0:T(1024)} %param.28) | copy-start | bytes 24580
Sparse Core Ops, SparseCore 0:
  11.0 73.3 all-gather.2
  87.3 67.1 all-gather.4
where the time goes:
time: 239 us; the launch traced here: 238 us
  waiting for transfers between devices  139 us (58%)
  matrix products  41.4 us (17%)
  local copies, waits for them, and re-layouts  28.5 us (12%)
  between operations  14.3 us (6%)
  starting transfers between devices  10.9 us (5%)
  other arithmetic  4.18 us (2%)
    all_gather x1, waiting for transfers between devices, body(): lax.all_gather(query_weight, 'ep', axis=1, tiled=True)  61 us
    all_gather x1, waiting for transfers between devices, body(): lax.all_gather(output_weight, 'ep', axis=1, tiled=True)  42.4 us
    all_to_all x1, waiting for transfers between devices, body(): lax.all_to_all(outgoing, 'ep', split_axis=0, concat_axis=0, tiled=True)  19 us
    all_to_all x1, waiting for transfers between devices, body(): lax.all_to_all(result.reshape(sources, count, features), 'ep', split_axis...  15.3 us
    unnamed x29, local copies, waits for them, and re-layouts  14.9 us
    dot_general x1, matrix products, body(): jnp.dot(attended, lax.all_gather(output_weight, 'ep', axis=1, tiled=True)...  5.76 us
    dot_general x1, matrix products, body(): jnp.dot(normed, lax.all_gather(query_weight, 'ep', axis=1, tiled=True), p...  5.65 us
    all_to_all x1, starting transfers between devices, body(): lax.all_to_all(result.reshape(sources, count, features), 'ep', split_axis...  5.44 us
  transfers between devices with their start and end apart: 4, of which 4 were waited for; matrix products, arithmetic and copies ran while one was open for 19% of the time, Pallas kernels for 0%

commit v1 on v0

--- a/solution.py
+++ b/solution.py
@@ -5,6 +5,11 @@
 from jax.sharding import PartitionSpec as P
 
 HD = 64
+
+
+def all_by_exchange(x, axis, along):
+    sent = jnp.stack([x] * lax.axis_size(axis))
+    return jnp.concatenate(lax.all_to_all(sent, axis, 0, 0), axis=along)
 
 
 def rms_scale(rows, gain):
@@ -56,9 +61,7 @@
         jnp.bfloat16
     )
     queries = jnp.dot(
-        normed,
-        lax.all_gather(query_weight, "ep", axis=1, tiled=True),
-        preferred_element_type=jnp.float32,
+        normed, all_by_exchange(query_weight, "ep", 1), preferred_element_type=jnp.float32
     ).astype(jnp.bfloat16)
     seqs, span, width = cache_keys.shape
     kv_heads = width // HD

time: 239 us -> 247 us (1.033)
  starting transfers between devices: 10.9 us -> 27 us
  waiting for transfers between devices: 139 us -> 126 us
  local copies, waits for them, and re-layouts: 28.5 us -> 32.9 us
    all_to_all x0 -> x1, waiting for transfers between devices: none -> 87.4 us  [all_by_exchange(): return jnp.concatenate(lax.all_to_all(sent, axis, 0, 0), axis=along)]
    all_gather x1 -> x0, waiting for transfers between devices: 61 us -> none  [body(): lax.all_gather(query_weight, 'ep', axis=1, tiled=True)]
    all_gather x1, waiting for transfers between devices: 42.4 us -> 3.16 us  [body(): lax.all_gather(output_weight, 'ep', axis=1, tiled=True)]
    all_to_all x0 -> x1, starting transfers between devices: none -> 11.9 us  [all_by_exchange(): return jnp.concatenate(lax.all_to_all(sent, axis, 0, 0), axis=along)]
    another operation x0 -> x1, local copies, waits for them, and re-layouts: none -> 5.12 us  [all_by_exchange(): sent = jnp.stack([x] * lax.axis_size(axis))]
    all_to_all x1, starting transfers between devices: 5.36 us -> 9.62 us  [body(): lax.all_to_all(outgoing, 'ep', split_axis=0, concat_axis=0, tiled=True)]
    unnamed x29 -> x31, local copies, waits for them, and re-layouts: 14.9 us -> 14.8 us
  transfers between devices with their start and end apart: 4 -> 4, of which waited for: 4 -> 4; matrix products, arithmetic and copies ran while one was open for 19% -> 21% of each run, Pallas kernels for 0% -> 0%
where the time goes in v1:
time: 247 us; the launch traced here: 246 us
  waiting for transfers between devices  126 us (51%)
  matrix products  41.8 us (17%)
  local copies, waits for them, and re-layouts  32.9 us (13%)
  starting transfers between devices  27 us (11%)
  between operations  14.3 us (6%)
  other arithmetic  4.18 us (2%)
    all_to_all x1, waiting for transfers between devices, all_by_exchange(): return jnp.concatenate(lax.all_to_all(sent, axis, 0, 0), axis=along)  87.4 us
    all_to_all x1, waiting for transfers between devices, body(): lax.all_to_all(outgoing, 'ep', split_axis=0, concat_axis=0, tiled=True)  19 us
    all_to_all x1, waiting for transfers between devices, body(): lax.all_to_all(result.reshape(sources, count, features), 'ep', split_axis...  15.3 us
    unnamed x31, local copies, waits for them, and re-layouts  14.8 us
    all_to_all x1, starting transfers between devices, all_by_exchange(): return jnp.concatenate(lax.all_to_all(sent, axis, 0, 0), axis=along)  11.9 us
    all_to_all x1, starting transfers between devices, body(): lax.all_to_all(outgoing, 'ep', split_axis=0, concat_axis=0, tiled=True)  9.62 us
    dot_general x1, matrix products, body(): jnp.einsum('skgl,slkd->skgd', stick, v_heads, preferred_element_type=jnp....  5.81 us
    dot_general x1, matrix products, body(): jnp.dot(attended, lax.all_gather(output_weight, 'ep', axis=1, tiled=True)...  5.76 us
  transfers between devices with their start and end apart: 4, of which 4 were waited for; matrix products, arithmetic and copies ran while one was open for 21% of the time, Pallas kernels for 0%

profile of v1, /device:TPU:1, one launch (start us, length us, event | category | flops | bytes accessed | tf_op | source)
XLA Modules:
  0.0 245.9 jit_solution(5244912437778920801)
XLA Ops:
  7.2 0.0 copy-start
  7.2 0.0 all-gather.2.cloned.1.call-start
  7.2 0.7 all-gather.2.cloned.1.call-update
  7.9 5.1 %stack.2 = bf16[128,2048,16]{1,2,0:T(8,128)(2,1)} broadcast(bf16[2048,16]{0,1:T(8,128)(2,1)} %param.29), dimensions={1,2} | broadcast | bytes 8454144 | tf_op jit(solution)/shard_map/stack | solution.py:11
  13.0 11.9 %all-to-all-start = ((bf16[128,2048,16]{1,2,0:T(8,128)(2,1)}), bf16[128,2048,16]{1,2,0:T(8,128)(2,1)}, u32[]{:S(2)}, u32[]{:S(2)}) async-start(bf16[128,2048,16]{1,2,0:T(8,128)(2,1)} %stack.2), calls=%async_computation | async-start | bytes 16777216 | tf_op jit(solution)/shard_map/all_to_all | solution.py:12
  25.0 0.0 copy-done.12
  25.0 0.1 add.115
  25.1 6.4 %copy.44 = bf16[16,1024,128]{1,2,0:T(8,128)(2,1)} copy(bf16[16,1024,128]{2,1,0:T(8,128)(2,1)} %param.23) | data formatting | bytes 8388608 | tf_op args[2]
  31.5 6.4 %copy.47 = bf16[16,1024,128]{1,2,0:T(8,128)(2,1)} copy(bf16[16,1024,128]{2,1,0:T(8,128)(2,1)} %param.24) | data formatting | bytes 8388608 | tf_op args[3]
  37.9 0.0 copy-done.9
  37.9 0.1 copy.48
  38.0 0.1 reshape.166
  38.1 0.3 fusion.13
  38.4 0.1 convert_element_type.88
  38.5 0.1 copy.50
  38.6 0.1 convert_reduce_fusion
  38.7 0.0 copy-done.1
  38.7 0.1 fusion.26
  38.9 0.0 copy-done.11
  38.9 0.1 iota_compare_fusion.2
  38.9 87.4 %all-to-all-done = bf16[128,2048,16]{1,2,0:T(8,128)(2,1)} async-done(((bf16[128,2048,16]{1,2,0:T(8,128)(2,1)}), bf16[128,2048,16]{1,2,0:T(8,128)(2,1)}, u32[]{:S(2)}, u32[]{:S(2)}) %all-to-all-start) | async-done | bytes 8388640 | tf_op jit(solution)/shard_map/all_to_all | solution.py:12
  126.4 0.0 copy-done.5
  126.4 5.6 %convolution_convert_fusion.3 = bf16[16,2048]{1,0:T(8,128)(2,1)S(1)} fusion(bf16[2048,2048]{0,1:T(8,128)(2,1)} %bitcast.1, bf16[16,2048]{1,0:T(8,128)(2,1)S(1)} %copy-done.1, f32[2048]{0:T(1024)S(1)} %copy-done.5, f32[16]{0:T(128)S(1)} %add_rsqrt_fusion.3), kind=kOutput, calls=%fused_computation.7 | convolution fusion | flops 134381568 | bytes 8527936 | tf_op jit(solution)/shard_map/dot_general | solution.py:63
  132.0 0.2 reshape.160
  132.2 5.3 %subtract_select_fusion = (f32[16,2,16,1024]{3,2,1,0:T(8,128)S(1)}, f32[16,2,16,1024]{3,2,1,0:T(8,128)}) fusion(f32[2,16]{1,0:T(2,128)S(1)} %add.115, pred[16,1024]{1,0:T(8,128)(4,1)S(1)} %iota_compare_fusion.2, bf16[16,2,16,64]{3,2,1,0:T(8,128)(2,1)S(1)} %reshape.160, bf16[16,1024,2,64]{1,3,2,0:T(8,128)(2,1)} %bitcast.67), kind=kOutput, calls=%fused_computation.15 | convolution fusion | flops 73400320 | bytes 8470656 | tf_op jit(solution)/shard_map/skgd,slkd->skgl/dot_general | solution.py:73
  137.5 1.8 copy.56
  139.3 2.2 reduce_sum.73
  141.5 0.2 fusion.40
  141.7 4.1 %convolution_add_fusion.1 = f32[16,2,16,8,128]{4,3,2,1,0:T(8,128)} fusion(f32[16,2,16,8,128]{4,3,2,1,0:T(8,128)} %bitcast.65, f32[16,2,16,8]{3,2,1,0:T(8,128)S(1)} %fusion.40), kind=kOutput, calls=%fused_computation.17 | convolution fusion | flops 805847040 | bytes 4210688 | tf_op jit(solution)/shard_map/skgbj,ji->skgbi/dot_general | solution.py:26
  145.8 2.7 %reshape.163 = f32[16,2,16,1024]{3,2,1,0:T(8,128)} reshape(f32[16,2,16,8,128]{4,3,2,1,0:T(8,128)} %convolution_add_fusion.1) | data formatting | bytes 4194304 | tf_op jit(solution)/shard_map/reshape | solution.py:31
  148.5 5.8 %convolution_convert_fusion.4 = bf16[16,2,16,64]{3,2,1,0:T(8,128)(2,1)S(1)} fusion(bf16[16,1024,2,64]{1,3,2,0:T(8,128)(2,1)} %bitcast.66, f32[16,2,16,1024]{3,2,1,0:T(8,128)} %reshape.163, f32[16,2,16,1024]{3,2,1,0:T(8,128)} %get-tuple-element.6, f32[2,16]{1,0:T(2,128)S(1)} %add.115, pred[16,1024]{1,0:T(8,128)(4,1)S(1)} %iota_compare_fusion.2), kind=kOutput, calls=%fused_computation.20 | convolution fusion | flops 73957376 | bytes 8470656 | tf_op jit(solution)/shard_map/skgl,slkd->skgd/dot_general | solution.py:82
  154.4 0.2 reshape.165
  154.5 0.0 copy-start.6
  154.6 0.0 copy-start.7
  154.6 3.2 %all-gather.2.cloned.1.call-done = bf16[2048,2048]{0,1:T(8,128)(2,1)} async-done(((bf16[2048,16]{0,1:T(8,128)(2,1)}), bf16[2048,2048]{0,1:T(8,128)(2,1)}) %all-gather.2.cloned.1.call-update) | async-done | bytes 8388624 | tf_op jit(solution)/shard_map/all_gather | solution.py:86
  157.7 5.8 %multiply_reduce_fusion.3 = (f32[16]{0:T(128)S(1)}, f32[16,2048]{1,0:T(8,128)S(1)}) fusion(bf16[16,2048]{1,0:T(8,128)(2,1)S(1)} %reshape.165, bf16[2048,2048]{0,1:T(8,128)(2,1)} %all-gather.2.cloned.1.call-done), kind=kOutput, calls=%fused_computation.47 | convolution fusion | flops 134348784 | bytes 8585280 | tf_op jit(solution)/shard_map/dot_general | solution.py:84
  163.5 0.0 copy-done.6
  163.5 0.2 multiply_reduce_fusion.2
  163.7 0.0 copy-done.7
  163.7 0.1 multiply_convert_fusion
  163.8 0.4 convolution_convert_fusion.1
  164.3 0.0 copy-start.10
  164.3 1.5 reshape.167
  165.8 9.6 %all-to-all-start.1 = ((bf16[128,2,2048]{2,1,0:T(2,128)(2,1)}), bf16[128,2,2048]{2,1,0:T(2,128)(2,1)S(1)}, u32[]{:S(2)}, u32[]{:S(2)}) async-start(bf16[128,2,2048]{2,1,0:T(2,128)(2,1)} %reshape.167), calls=%async_computation.1 | async-start | bytes 2097152 | tf_op jit(solution)/shard_map/all_to_all | solution.py:111
  175.5 0.1 mul.150
  175.5 0.1 copy.51
  175.6 19.0 %all-to-all-done.1 = bf16[128,2,2048]{2,1,0:T(2,128)(2,1)S(1)} async-done(((bf16[128,2,2048]{2,1,0:T(2,128)(2,1)}), bf16[128,2,2048]{2,1,0:T(2,128)(2,1)S(1)}, u32[]{:S(2)}, u32[]{:S(2)}) %all-to-all-start.1) | async-done | bytes 1048608 | tf_op jit(solution)/shard_map/all_to_all | solution.py:111
  194.7 1.2 reshape.168
  195.9 3.5 %fusion.5 = f32[256,512]{1,0:T(8,128)} fusion(bf16[256,2048]{1,0:T(8,128)(2,1)} %reshape.168, bf16[1,2048,512]{2,1,0:T(8,128)(2,1)} %param.36), kind=kOutput, calls=%fused_computation.12 | convolution fusion | flops 536870912 | bytes 3670016 | tf_op jit(solution)/shard_map/dot_general | solution.py:115
  199.4 0.0 copy-done.2
  199.4 4.0 %convolution_convert_fusion = bf16[256,2048]{1,0:T(8,128)(2,1)} fusion(bf16[1,512,2048]{2,1,0:T(8,128)(2,1)S(1)} %copy-done, bf16[256,2048]{1,0:T(8,128)(2,1)S(1)} %copy-done.2, bf16[1,2048,512]{2,1,0:T(8,128)(2,1)} %param.37, f32[256,512]{1,0:T(8,128)} %fusion.5), kind=kOutput, calls=%fused_computation.2 | convolution fusion | flops 1075052544 | bytes 6815744 | tf_op jit(solution)/shard_map/dot_general | solution.py:118
  203.4 2.6 %reshape.169 = bf16[128,2,2048]{2,1,0:T(2,128)(2,1)} reshape(bf16[256,2048]{1,0:T(8,128)(2,1)} %convolution_convert_fusion) | data formatting | bytes 2097152 | tf_op jit(solution)/shard_map/reshape | solution.py:122
  206.0 5.4 %all-to-all-start.2 = ((bf16[128,2,2048]{2,1,0:T(2,128)(2,1)}), bf16[128,2,2048]{2,1,0:T(2,128)(2,1)}, u32[]{:S(2)}, u32[]{:S(2)}) async-start(bf16[128,2,2048]{2,1,0:T(2,128)(2,1)} %reshape.169), calls=%async_computation.2 | async-start | bytes 2097152 | tf_op jit(solution)/shard_map/all_to_all | solution.py:121
  211.5 0.8 convolution_convert_fusion.5
  212.3 0.8 convolution_convert_fusion.6
  213.2 2.0 fusion.52
  215.1 15.3 %all-to-all-done.2 = bf16[128,2,2048]{2,1,0:T(2,128)(2,1)} async-done(((bf16[128,2,2048]{2,1,0:T(2,128)(2,1)}), bf16[128,2,2048]{2,1,0:T(2,128)(2,1)}, u32[]{:S(2)}, u32[]{:S(2)}) %all-to-all-start.2) | async-done | bytes 1048608 | tf_op jit(solution)/shard_map/all_to_all | solution.py:121
  230.4 1.5 reshape.170
  231.9 1.6 gather_fusion
  233.5 1.1 gather.7
  234.6 0.6 multiply_reduce_fusion
  235.2 0.0 copy-start.8
  235.2 3.1 %multiply_reduce_fusion.1 = (f32[16]{0:T(128)S(1)}, f32[16,2048]{1,0:T(8,128)S(1)}) fusion(f32[16,2048]{1,0:T(8,128)S(1)} %multiply_reduce_fusion, bf16[512,2048]{1,0:T(8,128)(2,1)} %param.41, bf16[16,2048]{1,0:T(8,128)(2,1)S(1)} %multiply_convert_fusion, bf16[2048,512]{1,0:T(8,128)(2,1)} %param.40, f32[16,512]{1,0:T(8,128)S(1)} %fusion.52), kind=kOutput, calls=%fused_computation.44 | convolution fusion | flops 67256304 | bytes 4554816 | tf_op jit(solution)/shard_map/dot_general | solution.py:110
  238.3 0.7 add_convert_fusion
  (22 shorter events, 0.1 us)
Async XLA Ops:
  7.2 192.2 %copy-start = (bf16[1,512,2048]{2,1,0:T(8,128)(2,1)S(1)}, bf16[1,512,2048]{2,1,0:T(8,128)(2,1)}, u32[]{:S(2)}) copy-start(bf16[1,512,2048]{2,1,0:T(8,128)(2,1)} %param.38) | copy-start | bytes 6291460
  7.2 150.5 %all-gather.2.cloned.1.call-start = ((), (), s32[]{:S(2)}) async-start(), calls=%async_computation.3 | async-start | bytes 8454144 | tf_op jit(solution)/shard_map/all_gather | solution.py:86
  13.0 12.0 %copy-start.12 = (f32[32]{0:T(128)S(1)}, f32[32]{0:T(128)}, u32[]{:S(2)}) copy-start(f32[32]{0:T(128)} %param.32) | copy-start | bytes 388
  13.0 113.3 %all-to-all-start = ((bf16[128,2048,16]{1,2,0:T(8,128)(2,1)}), bf16[128,2048,16]{1,2,0:T(8,128)(2,1)}, u32[]{:S(2)}, u32[]{:S(2)}) async-start(bf16[128,2048,16]{1,2,0:T(8,128)(2,1)} %stack.2), calls=%async_computation | async-start | bytes 16777216 | tf_op jit(solution)/shard_map/all_to_all | solution.py:12
  31.5 6.5 %copy-start.9 = (s32[16,6]{0,1:T(8,128)S(1)}, s32[16,6]{0,1:T(8,128)}, u32[]{:S(2)}) copy-start(s32[16,6]{0,1:T(8,128)} %param.34) | copy-start | bytes 1156
  31.5 7.2 %copy-start.1 = (bf16[16,2048]{1,0:T(8,128)(2,1)S(1)}, bf16[16,2048]{1,0:T(8,128)(2,1)}, u32[]{:S(2)}) copy-start(bf16[16,2048]{1,0:T(8,128)(2,1)} %param.21) | copy-start | bytes 196612
  31.5 7.4 %copy-start.11 = (s32[16]{0:T(128)S(1)}, s32[16]{0:T(128)}, u32[]{:S(2)}) copy-start(s32[16]{0:T(128)} %param.22) | copy-start | bytes 196
  31.5 94.9 %copy-start.5 = (f32[2048]{0:T(1024)S(1)}, f32[2048]{0:T(1024)}, u32[]{:S(2)}) copy-start(f32[2048]{0:T(1024)} %param.25) | copy-start | bytes 24580
  154.5 9.0 %copy-start.6 = (f32[2048]{0:T(1024)S(1)}, f32[2048]{0:T(1024)}, u32[]{:S(2)}) copy-start(f32[2048]{0:T(1024)} %param.26) | copy-start | bytes 24580
  154.6 9.2 %copy-start.7 = (f32[2048]{0:T(1024)S(1)}, f32[2048]{0:T(1024)}, u32[]{:S(2)}) copy-start(f32[2048]{0:T(1024)} %param.27) | copy-start | bytes 24580
  164.3 11.2 %copy-start.10 = (f32[16,6]{0,1:T(8,128)S(1)}, f32[16,6]{0,1:T(8,128)}, u32[]{:S(2)}) copy-start(f32[16,6]{0,1:T(8,128)} %param.35) | copy-start | bytes 1156
  165.8 28.9 %all-to-all-start.1 = ((bf16[128,2,2048]{2,1,0:T(2,128)(2,1)}), bf16[128,2,2048]{2,1,0:T(2,128)(2,1)S(1)}, u32[]{:S(2)}, u32[]{:S(2)}) async-start(bf16[128,2,2048]{2,1,0:T(2,128)(2,1)} %reshape.167), calls=%async_computation.1 | async-start | bytes 2097152 | tf_op jit(solution)/shard_map/all_to_all | solution.py:111
  195.9 3.5 %copy-start.2 = (bf16[256,2048]{1,0:T(8,128)(2,1)S(1)}, bf16[256,2048]{1,0:T(8,128)(2,1)}, u32[]{:S(2)}) copy-start(bf16[256,2048]{1,0:T(8,128)(2,1)} %reshape.168) | copy-start | bytes 3145732
  203.4 8.1 %copy-start.3 = (bf16[2048,128]{1,0:T(8,128)(2,1)S(1)}, bf16[2048,128]{1,0:T(8,128)(2,1)}, u32[]{:S(2)}) copy-start(bf16[2048,128]{1,0:T(8,128)(2,1)} %param.31) | copy-start | bytes 1572868
  203.4 9.0 %copy-start.4 = (bf16[2048,128]{1,0:T(8,128)(2,1)S(1)}, bf16[2048,128]{1,0:T(8,128)(2,1)}, u32[]{:S(2)}) copy-start(bf16[2048,128]{1,0:T(8,128)(2,1)} %param.30) | copy-start | bytes 1572868
  206.0 24.5 %all-to-all-start.2 = ((bf16[128,2,2048]{2,1,0:T(2,128)(2,1)}), bf16[128,2,2048]{2,1,0:T(2,128)(2,1)}, u32[]{:S(2)}, u32[]{:S(2)}) async-start(bf16[128,2,2048]{2,1,0:T(2,128)(2,1)} %reshape.169), calls=%async_computation.2 | async-start | bytes 2097152 | tf_op jit(solution)/shard_map/all_to_all | solution.py:121
  235.2 3.1 %copy-start.8 = (f32[2048]{0:T(1024)S(1)}, f32[2048]{0:T(1024)}, u32[]{:S(2)}) copy-start(f32[2048]{0:T(1024)} %param.28) | copy-start | bytes 24580
Sparse Core Ops, SparseCore 0:
  11.0 146.7 all-gather.1
